TPU v7x, 256 devices: a whole 4x4x8 slice. The times are simulated.
256 devices in a mesh: sp: 16 (over y, x), tp: 16 (over z, core).
Axes of the slice: x: 4, y: 4, z: 8, core: 2. Of those that a mesh axis runs over, the one named last changes fastest.
Arguments:
- residual: bfloat16 [8192, 2048], P(('sp', 'tp')), may hold values from -6 to 6
- queries: bfloat16 [8192, 4096], P('sp', 'tp'), may hold values from -6 to 6
- keys: bfloat16 [8192, 4096], P('sp', 'tp'), may hold values from -6 to 6
- values: bfloat16 [8192, 4096], P('sp', 'tp'), may hold values from -6 to 6
- in_gate: float32 [16, 8192], P('tp', 'sp'), may hold values from -5 to 130
- forget_gate: float32 [16, 8192], P('tp', 'sp'), may hold values from 0 to 16
- doc_ids: int32 [8192], P('sp'), may hold values from 0 to 7, never falling along the last dimension, each value on 1 to 4096 neighbouring positions
- head_gain: float32 [4096], P('tp'), may hold values from 0.1 to 1.9
- out_weight: bfloat16 [4096, 2048], P('tp'), may hold values from -0.09375 to 0.09375
- norm_gain: float32 [2048], replicated, may hold values from 0.1 to 1.9
- route_ids: int32 [8192, 2], P(('sp', 'tp')), may hold values from 0 to 15, all different within a row; in each aligned block of 32 rows (0 to 31, 32 to 63, ...) at most 5 rows name the same one
- route_weights: float32 [8192, 2], P(('sp', 'tp')), may hold values from 0.2 to 1
- gate_proj: bfloat16 [16, 2048, 4096], P('sp', None, 'tp'), may hold values from -0.125 to 0.125
- up_proj: bfloat16 [16, 2048, 4096], P('sp', None, 'tp'), may hold values from -0.125 to 0.125
- down_proj: bfloat16 [16, 4096, 2048], P('sp', 'tp'), may hold values from -0.09375 to 0.09375
Outputs:
- mixed: bfloat16 [8192, 2048], P(('sp', 'tp'))
Inputs may be any that keep to these rules, and one draw needn't show every extreme that they name: `route_ids`: each row names 2 different experts. In each aligned block of 32 rows (the rows of one device) no expert is named by more than 5 rows, and in some blocks one expert by exactly 5. `doc_ids`: numbers never fall along the sequence; no document covers more than half of the 8192 positions, and one covers exactly half.
All inputs are finite; a program needn't handle non-finite values.
Results may differ from a plain program's by a relative error of at most 0.018.
Values may be sent and summed in bfloat16 or wider, within the bound.
A program may use at most 64 MiB of HBM per device.

v0:
```python
import math
import jax
import jax.numpy as jnp
from jax import lax
from jax.sharding import Mesh
from jax.sharding import PartitionSpec as P

SP = ("sp_0", "sp_1")
SP_TP = ("sp_0", "sp_1", "tp")
MASKED = -1e30
EPSILON = 1e-06


def neutral_like(value, identity):
    return jax.tree.map(
        lambda a, e: jnp.broadcast_to(jnp.asarray(e, a.dtype), a.shape), value, identity
    )


def carried_in(value, axes, combine, identity):
    before = start = neutral_like(value, identity)
    running = value
    for axis in reversed(axes):
        peers, index = (lax.axis_size(axis), lax.axis_index(axis))
        pieces = jax.tree.map(lambda part: lax.all_gather(part, axis), running)
        inside, running = (start, start)
        for k in range(peers):
            passed = k < index
            running = combine(running, jax.tree.map(lambda part: part[k], pieces))
            inside = jax.tree.map(lambda new, old: jnp.where(passed, new, old), running, inside)
        before = combine(inside, before)
    return before


def block_step(state, pieces):
    memory, normalizer, max_level, carry_doc = state
    q_block, k_block, v_block, in_block, forget_block, doc_block = pieces
    scaling = q_block.shape[1] ** (-0.5)
    cum_forget = jnp.cumsum(forget_block)
    positions = jnp.arange(q_block.shape[0])
    permitted_mask = (positions[:, None] >= positions[None, :]) & (
        doc_block[:, None] == doc_block[None, :]
    )
    log_weights = jnp.where(
        permitted_mask, cum_forget[:, None] - cum_forget[None, :] + in_block[None, :], MASKED
    )
    carried = jnp.where(doc_block == carry_doc, cum_forget + max_level, MASKED)
    row_max = jnp.maximum(carried, jnp.max(log_weights, axis=1))
    scores = jnp.dot(q_block, k_block.T, preferred_element_type=jnp.float32) * scaling
    weighted = scores * jnp.exp(log_weights - row_max[:, None])
    carry_weight = jnp.exp(carried - row_max)
    query_scaled = q_block.astype(jnp.float32) * scaling
    key_full = k_block.astype(jnp.float32)
    value_full = v_block.astype(jnp.float32)
    readout_numerator = jnp.dot(weighted, value_full, precision=lax.Precision.HIGHEST)
    readout_numerator = readout_numerator + carry_weight[:, None] * jnp.dot(
        query_scaled, memory.T, precision=lax.Precision.HIGHEST
    )
    denominator = jnp.sum(weighted, axis=1) + carry_weight * jnp.dot(
        query_scaled, normalizer, precision=lax.Precision.HIGHEST
    )
    last_doc = doc_block[-1]
    forget_total = cum_forget[-1]
    log_end = jnp.where(doc_block == last_doc, forget_total - cum_forget + in_block, MASKED)
    carry_log = jnp.where(carry_doc == last_doc, forget_total + max_level, MASKED)
    new_max = jnp.maximum(carry_log, jnp.max(log_end))
    end_weight = jnp.exp(log_end - new_max)
    kept_share = jnp.exp(carry_log - new_max)
    new_memory = kept_share * memory + jnp.dot(
        (value_full * end_weight[:, None]).T, key_full, precision=lax.Precision.HIGHEST
    )
    new_normalizer = kept_share * normalizer + jnp.dot(
        end_weight, key_full, precision=lax.Precision.HIGHEST
    )
    return (
        (new_memory, new_normalizer, new_max, last_doc),
        (readout_numerator, denominator, row_max),
    )


def run_blocks(
    queries_in,
    keys_in,
    incoming_vectors,
    in_gates,
    log_forget,
    doc_row,
    memory,
    normalizer,
    max_level,
    carry_doc,
):
    extent = queries_in.shape[0]
    block_size = math.gcd(extent, 256)
    blocks = extent // block_size

    def to_blocks(tensor):
        return tensor.reshape((blocks, block_size) + tensor.shape[1:])

    pieces = tuple(
        (
            to_blocks(tensor)
            for tensor in (queries_in, keys_in, incoming_vectors, in_gates, log_forget, doc_row)
        )
    )
    final_state, outputs = lax.scan(block_step, (memory, normalizer, max_level, carry_doc), pieces)
    readout_numerator, denominator, row_max = outputs
    return (
        readout_numerator.reshape(extent, -1),
        denominator.reshape(extent),
        row_max.reshape(extent),
        final_state,
    )


def combine_states(earlier, later):
    memory_a, normal_a, level_a, forget_a, first_a, last_a = earlier
    memory_b, normal_b, level_b, forget_b, first_b, last_b = later
    joined = (last_a == first_b) | (last_a < 0) | (first_b < 0)
    passed = forget_b + jnp.where(joined, 0.0, MASKED)
    new_level = jnp.maximum(passed + level_a, level_b)
    share_a = jnp.exp(passed + level_a - new_level)
    fraction_second = jnp.exp(level_b - new_level)
    new_memory = share_a[:, None, None] * memory_a + fraction_second[:, None, None] * memory_b
    new_normal = share_a[:, None] * normal_a + fraction_second[:, None] * normal_b
    first_doc = jnp.where(first_a < 0, first_b, first_a)
    last_doc = jnp.where(last_b < 0, last_a, last_b)
    return (new_memory, new_normal, new_level, forget_a + passed, first_doc, last_doc)


def on_device(
    residual,
    queries,
    keys,
    values,
    in_gate,
    forget_gate,
    doc_ids,
    head_gain,
    out_weight,
    norm_gain,
    route_ids,
    route_weights,
    gate_proj,
    up_proj,
    down_proj,
):
    extent, local_width = queries.shape
    heads_here = in_gate.shape[0]
    head_size = local_width // heads_here

    def by_head(tensor):
        return tensor.reshape(extent, heads_here, head_size).transpose(1, 0, 2)

    query_heads = by_head(queries)
    key_heads = by_head(keys)
    value_heads = by_head(values)
    log_forget = jax.nn.log_sigmoid(forget_gate)
    cum_forget = jnp.cumsum(log_forget, axis=1)
    first_doc = doc_ids[0]
    last_doc = doc_ids[-1]
    run_heads = jax.vmap(run_blocks, in_axes=(0, 0, 0, 0, 0, None, 0, 0, 0, None))
    forget_total = jnp.where(first_doc == last_doc, cum_forget[:, -1], MASKED)
    doc_first = first_doc.astype(jnp.float32).reshape(1)
    doc_last = last_doc.astype(jnp.float32).reshape(1)
    empty_memory = jnp.zeros((heads_here, head_size, head_size), jnp.float32)
    empty_normal = jnp.zeros((heads_here, head_size), jnp.float32)
    empty_level = jnp.full((heads_here,), MASKED, jnp.float32)
    identity = (
        empty_memory,
        empty_normal,
        empty_level,
        jnp.zeros((heads_here,), jnp.float32),
        jnp.full((1,), -1.0, jnp.float32),
        jnp.full((1,), -1.0, jnp.float32),
    )
    readout_numerator, denominator, row_max, final_state = run_heads(
        query_heads,
        key_heads,
        value_heads,
        in_gate,
        log_forget,
        doc_ids,
        empty_memory,
        empty_normal,
        empty_level,
        first_doc,
    )
    local_state = (
        final_state[0],
        final_state[1],
        final_state[2],
        forget_total,
        doc_first,
        doc_last,
    )
    incoming = carried_in(local_state, SP, combine_states, identity)
    linked = incoming[5][0] == doc_first[0]
    in_level = jnp.where(linked, incoming[2], MASKED)
    carried = jnp.where(doc_ids[None, :] == first_doc, cum_forget + in_level[:, None], MASKED)
    new_max = jnp.maximum(row_max, carried)
    own_share = jnp.exp(row_max - new_max)
    far_share = jnp.exp(carried - new_max)
    query_scaled = query_heads.astype(jnp.float32) * head_size ** (-0.5)
    readout_numerator = own_share[..., None] * readout_numerator + far_share[
        ..., None
    ] * jnp.einsum("htd,hvd->htv", query_scaled, incoming[0], precision=lax.Precision.HIGHEST)
    denominator = own_share * denominator + far_share * jnp.einsum(
        "htd,hd->ht", query_scaled, incoming[1], precision=lax.Precision.HIGHEST
    )
    mixed_heads = (
        readout_numerator / jnp.maximum(jnp.abs(denominator), jnp.exp(-new_max))[..., None]
    )
    normed_heads = mixed_heads * lax.rsqrt(
        jnp.mean(mixed_heads * mixed_heads, axis=-1, keepdims=True) + EPSILON
    )
    normed_heads = normed_heads * head_gain.reshape(heads_here, 1, head_size)
    head_rows = normed_heads.transpose(1, 0, 2).reshape(extent, local_width).astype(jnp.bfloat16)
    rows_here, model_width = residual.shape
    update = lax.psum_scatter(
        jnp.dot(head_rows, out_weight, preferred_element_type=jnp.float32).astype(jnp.bfloat16),
        "tp",
        scatter_dimension=0,
        tiled=True,
    ).astype(jnp.float32)
    stream = residual.astype(jnp.float32) + update
    normed = (
        stream * lax.rsqrt(jnp.mean(stream * stream, axis=-1, keepdims=True) + EPSILON) * norm_gain
    )
    normed = normed.astype(jnp.bfloat16)
    experts_all = gate_proj.shape[0] * lax.axis_size(SP)
    top_count = route_ids.shape[1]
    capacity = max(2, rows_here * top_count * 5 // (4 * experts_all))
    flat_ids = route_ids.reshape(-1)
    onehot = (flat_ids[:, None] == jnp.arange(experts_all, dtype=jnp.int32)[None, :]).astype(
        jnp.int32
    )
    earlier = jnp.cumsum(onehot, axis=0) - onehot
    slot_rank = jnp.sum(earlier * onehot, axis=1)
    slot_index = flat_ids * capacity + slot_rank
    placing = (
        slot_index[None, :] == jnp.arange(experts_all * capacity, dtype=jnp.int32)[:, None]
    ).astype(jnp.bfloat16)
    copies = jnp.repeat(normed, top_count, axis=0)
    outgoing = jnp.dot(placing, copies, preferred_element_type=jnp.float32).astype(jnp.bfloat16)
    outgoing = outgoing.reshape(experts_all, capacity, model_width)
    arrived = lax.all_to_all(outgoing, SP, split_axis=0, concat_axis=0, tiled=True).reshape(
        -1, model_width
    )
    piece = lax.all_gather(arrived, "tp", axis=0, tiled=True)
    gate_part = jnp.dot(piece, gate_proj[0], preferred_element_type=jnp.float32)
    up_part = jnp.dot(piece, up_proj[0], preferred_element_type=jnp.float32)
    hidden = (jax.nn.silu(gate_part) * up_part).astype(jnp.bfloat16)
    expert_sum = lax.psum_scatter(
        jnp.dot(hidden, down_proj[0], preferred_element_type=jnp.float32).astype(jnp.bfloat16),
        "tp",
        scatter_dimension=0,
        tiled=True,
    )
    expert_out = expert_sum.reshape(experts_all, capacity, model_width)
    returned = lax.all_to_all(expert_out, SP, split_axis=0, concat_axis=0, tiled=True)
    picked = jnp.take(returned.reshape(-1, model_width), slot_index, axis=0)
    picked = picked.reshape(rows_here, top_count, model_width)
    expert_mix = jnp.sum(route_weights[..., None] * picked.astype(jnp.float32), axis=1)
    return (stream + expert_mix).astype(jnp.bfloat16)


def solution(mesh):
    finer = Mesh(mesh.devices.reshape(4, 4, mesh.shape["tp"]), ("sp_0", "sp_1", "tp"))
    in_specs = (
        P(SP_TP, None),
        P(SP, "tp"),
        P(SP, "tp"),
        P(SP, "tp"),
        P("tp", SP),
        P("tp", SP),
        P(SP),
        P("tp"),
        P("tp", None),
        P(),
        P(SP_TP, None),
        P(SP_TP, None),
        P(SP, None, "tp"),
        P(SP, None, "tp"),
        P(SP, "tp", None),
    )
    out_specs = P(SP_TP, None)
    return jax.shard_map(
        on_device, mesh=finer, in_specs=in_specs, out_specs=out_specs, check_vma=False
    )
```

profile of v0, /device:TPU:2, one launch (start us, length us, event | category | flops | bytes accessed | tf_op | source)
XLA Modules:
  0.0 372.2 jit_solution(4518122679349654062)
XLA Ops:
  10.0 25.1 %while.23 = (s32[]{:T(128)}, f32[1,256,256]{2,1,0:T(8,128)S(1)}, f32[1,256]{1,0:T(1,128)S(1)}, f32[1]{0:T(128)}, s32[]{:T(128)}, /*index=5*/f32[2,1,256,256]{3,2...) while((s32[]{:T(128)}, f32[1,256,256]{2,1,0:T(8,128)S(1)}, ...), condition=%wide.region_6.7_spmd.clone, body=%wide.region_0.6_spmd.clone.sunk | while | flops 641046528 | bytes 6349332 | solution.py:106
  15.7 1.9 fusion.223
  28.2 1.9 fusion.223
  45.2 10.0 %all-reduce.8 = (f32[4]{0:T(128)S(1)}, f32[4]{0:T(128)S(1)}, f32[4]{0:T(128)S(1)}, f32[4]{0:T(128)S(1)}) all-reduce(f32[4]{0:T(128)S(1)} %dynamic-update-slice, f32[4]{0:T(128)S(1)} %fusion.156, f32[4]{0:T(128)S(1)} %dynamic-update-slice.3, f32[4]{0:T(128)S(1)} %dynamic-update-slice.6), channel_id=1, replica_groups=mesh['sp_0'=4,'sp_1'=4,'tp'=16] {'sp_1'}, use_global_device_ids=true, to_apply=%add | all-reduce | flops 16 | bytes 128
  55.9 2.6 fusion.152
  72.3 2.0 fusion.70
  75.1 1.9 fusion.188
  80.3 1.4 dynamic-update-slice.5
  81.8 1.4 dynamic-update-slice.1
  83.2 9.3 %all-reduce.9 = (f32[4]{0:T(128)S(1)}, f32[4]{0:T(128)S(1)}, f32[4]{0:T(128)S(1)}, f32[4]{0:T(128)S(1)}) all-reduce(f32[4]{0:T(128)S(1)} %dynamic-update-slice.1, f32[4]{0:T(128)S(1)} %dynamic-update-slice.4, f32[4]{0:T(128)S(1)} %dynamic-update-slice.5, f32[4]{0:T(128)S(1)} %dynamic-update-slice.7), channel_id=2, replica_groups=mesh['sp_0'=4,'sp_1'=4,'tp'=16] {'sp_0'}, use_global_device_ids=true, to_apply=%add.1 | all-reduce | flops 16 | bytes 128
  121.3 9.6 %all-gather.8 = f32[4,1,256]{2,1,0:T(1,128)S(1)} all-gather(f32[1,1,256]{2,1,0:T(1,128)S(1)} %bitcast.322), channel_id=9, replica_groups=mesh['sp_0'=4,'sp_1'=4,'tp'=16] {'sp_1'}, dimensions={0}, use_global_device_ids=true | all-gather | bytes 5120 | tf_op jit(solution)/shard_map/all_gather | solution.py:25
  130.9 7.0 %all_gather.84 = f32[4,1,256]{2,1,0:T(1,128)S(1)} all-gather(f32[1,1,256]{2,1,0:T(1,128)S(1)} %get-tuple-element.176), channel_id=1, replica_groups=mesh['sp_0'=4,'sp_1'=4,'tp'=16] {'sp_0'}, dimensions={0}, use_global_device_ids=true | all-gather | bytes 5120 | tf_op jit(solution)/shard_map/all_gather | solution.py:25
  139.3 2.6 multiply_reduce_fusion.1
  141.9 2.2 convolution_convert_fusion.1
  144.7 59.9 %reduce-scatter.3.cloned.1.call-done = bf16[32,2048]{1,0:T(8,128)(2,1)} async-done(((bf16[512,2048]{1,0:T(8,128)(2,1)}), bf16[32,2048]{1,0:T(8,128)(2,1)}) %reduce-scatter.3.cloned.1.call-update) | async-done | bytes 131088 | tf_op jit(solution)/shard_map/reduce_scatter | solution.py:220
  207.4 15.9 %all_to_all.10 = bf16[16,5,2048]{2,1,0:T(8,128)(2,1)S(1)} all-to-all(bf16[16,5,2048]{2,1,0:T(8,128)(2,1)S(1)} %reshape.898), channel_id=1, replica_groups=mesh['sp_0'=4,'sp_1'=4,'tp'=16] {'sp_0','sp_1'}, dimensions={0} | all-to-all | bytes 655360 | tf_op jit(solution)/shard_map/all_to_all | solution.py:247
  224.4 40.1 %all-gather.15.cloned.1.call-done = bf16[1280,2048]{1,0:T(8,128)(2,1)} async-done(((bf16[80,2048]{1,0:T(8,128)(2,1)}), bf16[1280,2048]{1,0:T(8,128)(2,1)}) %all-gather.15.cloned.1.call-update) | async-done | bytes 5242896 | tf_op jit(solution)/shard_map/all_gather | solution.py:250
  264.5 5.1 %fusion.56 = f32[1280,256]{1,0:T(8,128)} fusion(bf16[1280,2048]{1,0:T(8,128)(2,1)} %all-gather.15.cloned.1.call-done, bf16[1,2048,256]{2,1,0:T(8,128)(2,1)S(1)} %copy-done.14), kind=kOutput, calls=%fused_computation.85 | convolution fusion | flops 1342177280 | bytes 7602176 | tf_op jit(solution)/shard_map/dot_general | solution.py:251
  269.6 10.6 %convolution_convert_fusion = bf16[1280,2048]{1,0:T(8,128)(2,1)} fusion(bf16[1280,2048]{1,0:T(8,128)(2,1)} %all-gather.15.cloned.1.call-done, f32[1280,256]{1,0:T(8,128)} %fusion.56, bf16[1,256,2048]{2,1,0:T(8,128)(2,1)S(1)} %copy-done, bf16[1,2048,256]{2,1,0:T(8,128)(2,1)S(1)} %copy-done.15), kind=kOutput, calls=%fused_computation.75 | convolution fusion | flops 2688942080 | bytes 13893632 | tf_op jit(solution)/shard_map/dot_general | solution.py:255
  280.9 63.2 %reduce-scatter.5.cloned.1.call-done = bf16[80,2048]{1,0:T(8,128)(2,1)} async-done(((bf16[1280,2048]{1,0:T(8,128)(2,1)}), bf16[80,2048]{1,0:T(8,128)(2,1)}) %reduce-scatter.5.cloned.1.call-update) | async-done | bytes 327696 | tf_op jit(solution)/shard_map/reduce_scatter | solution.py:254
  344.2 1.9 reshape.900
  346.1 7.3 %all-to-all-start.1 = ((bf16[16,5,2048]{2,1,0:T(8,128)(2,1)}), bf16[16,5,2048]{2,1,0:T(8,128)(2,1)S(1)}, u32[]{:S(2)}, u32[]{:S(2)}) async-start(bf16[16,5,2048]{2,1,0:T(8,128)(2,1)} %reshape.900), calls=%async_computation.3 | async-start | bytes 1048576 | tf_op jit(solution)/shard_map/all_to_all | solution.py:261
  353.4 8.7 %all-to-all-done.1 = bf16[16,5,2048]{2,1,0:T(8,128)(2,1)S(1)} async-done(((bf16[16,5,2048]{2,1,0:T(8,128)(2,1)}), bf16[16,5,2048]{2,1,0:T(8,128)(2,1)S(1)}, u32[]{:S(2)}, u32[]{:S(2)}) %all-to-all-start.1) | async-done | bytes 327712 | tf_op jit(solution)/shard_map/all_to_all | solution.py:261
  363.2 1.8 multiply_reduce_fusion
  (169 shorter events, 42.9 us)
Async XLA Ops:
  6.5 263.0 %copy-start = (bf16[1,256,2048]{2,1,0:T(8,128)(2,1)S(1)}, bf16[1,256,2048]{2,1,0:T(8,128)(2,1)}, u32[]{:S(2)}) copy-start(bf16[1,256,2048]{2,1,0:T(8,128)(2,1)} %param.31) | copy-start | bytes 3145732
  6.5 65.7 %all-gather.17.cloned.1.call-start = ((), (), s32[]{:S(2)}) async-start(), calls=%async_computation.8 | async-start | bytes 1310720 | tf_op jit(solution)/shard_map/all_gather | solution.py:25
  10.0 31.6 %copy-start.17 = (u32[256]{0:T(256)S(1)}, u32[256]{0:T(256)}, u32[]{:S(2)}) copy-start(u32[256]{0:T(256)} %constant.127) | copy-start | bytes 3076
  10.0 64.3 %copy-start.16 = (u32[256]{0:T(256)S(1)}, u32[256]{0:T(256)}, u32[]{:S(2)}) copy-start(u32[256]{0:T(256)} %constant.132) | copy-start | bytes 3076
  10.1 10.8 %copy-start.4 = (bf16[2,1,256,256]{3,2,1,0:T(8,128)(2,1)S(1)}, bf16[2,1,256,256]{3,2,1,0:T(8,128)(2,1)}, u32[]{:S(2)}) copy-start(bf16[2,1,256,256]{3,2,1,0:T(8,128)(2,1)} %get-tuple-element.388) | copy-start | bytes 786436 | tf_op jit(solution)/shard_map/vmap()/while
  10.1 10.8 %copy-start.5 = (bf16[2,1,256,256]{3,2,1,0:T(8,128)(2,1)S(1)}, bf16[2,1,256,256]{3,2,1,0:T(8,128)(2,1)}, u32[]{:S(2)}) copy-start(bf16[2,1,256,256]{3,2,1,0:T(8,128)(2,1)} %get-tuple-element.387) | copy-start | bytes 786436 | tf_op jit(solution)/shard_map/vmap()/while
  10.1 11.3 %copy-start.2 = (bf16[2,1,256,256]{3,2,1,0:T(8,128)(2,1)S(1)}, bf16[2,1,256,256]{3,2,1,0:T(8,128)(2,1)}, u32[]{:S(2)}) copy-start(bf16[2,1,256,256]{3,2,1,0:T(8,128)(2,1)} %get-tuple-element.389) | copy-start | bytes 786436 | tf_op jit(solution)/shard_map/vmap()/while
  22.6 10.8 %copy-start.4 = (bf16[2,1,256,256]{3,2,1,0:T(8,128)(2,1)S(1)}, bf16[2,1,256,256]{3,2,1,0:T(8,128)(2,1)}, u32[]{:S(2)}) copy-start(bf16[2,1,256,256]{3,2,1,0:T(8,128)(2,1)} %get-tuple-element.388) | copy-start | bytes 786436 | tf_op jit(solution)/shard_map/vmap()/while
  22.6 10.8 %copy-start.5 = (bf16[2,1,256,256]{3,2,1,0:T(8,128)(2,1)S(1)}, bf16[2,1,256,256]{3,2,1,0:T(8,128)(2,1)}, u32[]{:S(2)}) copy-start(bf16[2,1,256,256]{3,2,1,0:T(8,128)(2,1)} %get-tuple-element.387) | copy-start | bytes 786436 | tf_op jit(solution)/shard_map/vmap()/while
  22.6 11.3 %copy-start.2 = (bf16[2,1,256,256]{3,2,1,0:T(8,128)(2,1)S(1)}, bf16[2,1,256,256]{3,2,1,0:T(8,128)(2,1)}, u32[]{:S(2)}) copy-start(bf16[2,1,256,256]{3,2,1,0:T(8,128)(2,1)} %get-tuple-element.389) | copy-start | bytes 786436 | tf_op jit(solution)/shard_map/vmap()/while
  35.1 102.7 %copy-start.9 = (s32[512]{0:T(512)S(1)}, s32[512]{0:T(512)}, u32[]{:S(2)}) copy-start(s32[512]{0:T(512)} %param.23) | copy-start | bytes 6148
  35.2 103.5 %copy-start.3 = (bf16[2,1,256,256]{3,2,1,0:T(8,128)(2,1)S(1)}, bf16[2,1,256,256]{3,2,1,0:T(8,128)(2,1)}, u32[]{:S(2)}) copy-start(bf16[2,1,256,256]{3,2,1,0:T(8,128)(2,1)} %get-tuple-element.404) | copy-start | bytes 786436
  35.9 103.4 %all-gather.13.cloned.1.call-start = ((), (), s32[]{:S(2)}) async-start(), calls=%async_computation.4 | async-start | bytes 1310720 | tf_op jit(solution)/shard_map/all_gather | solution.py:25
  74.3 130.3 %reduce-scatter.3.cloned.1.call-start = ((), (), s32[]{:S(2)}) async-start(), calls=%async_computation.5 | async-start | bytes 2228224 | tf_op jit(solution)/shard_map/reduce_scatter | solution.py:220
  139.3 2.6 copy-start.8
  139.3 2.6 copy-start.13
  141.9 62.7 %copy-start.6 = (bf16[32,2048]{1,0:T(8,128)(2,1)S(1)}, bf16[32,2048]{1,0:T(8,128)(2,1)}, u32[]{:S(2)}) copy-start(bf16[32,2048]{1,0:T(8,128)(2,1)} %param.17) | copy-start | bytes 393220
  144.1 61.6 %copy-start.11 = (f32[2048]{0:T(1024)S(1)}, f32[2048]{0:T(1024)}, u32[]{:S(2)}) copy-start(f32[2048]{0:T(1024)} %param.26) | copy-start | bytes 24580
  144.1 120.3 %all-gather.15.cloned.1.call-start = ((), (), s32[]{:S(2)}) async-start(), calls=%async_computation.6 | async-start | bytes 5570560 | tf_op jit(solution)/shard_map/all_gather | solution.py:250
  206.9 57.6 %copy-start.14 = (bf16[1,2048,256]{2,1,0:T(8,128)(2,1)S(1)}, bf16[1,2048,256]{2,1,0:T(8,128)(2,1)}, u32[]{:S(2)}) copy-start(bf16[1,2048,256]{2,1,0:T(8,128)(2,1)} %param.29) | copy-start | bytes 3145732
  224.1 45.4 %copy-start.15 = (bf16[1,2048,256]{2,1,0:T(8,128)(2,1)S(1)}, bf16[1,2048,256]{2,1,0:T(8,128)(2,1)}, u32[]{:S(2)}) copy-start(bf16[1,2048,256]{2,1,0:T(8,128)(2,1)} %param.30) | copy-start | bytes 3145732
  224.2 120.0 %reduce-scatter.5.cloned.1.call-start = ((), (), s32[]{:S(2)}) async-start(), calls=%async_computation.7 | async-start | bytes 5570560 | tf_op jit(solution)/shard_map/reduce_scatter | solution.py:254
  346.1 16.1 %all-to-all-start.1 = ((bf16[16,5,2048]{2,1,0:T(8,128)(2,1)}), bf16[16,5,2048]{2,1,0:T(8,128)(2,1)S(1)}, u32[]{:S(2)}, u32[]{:S(2)}) async-start(bf16[16,5,2048]{2,1,0:T(8,128)(2,1)} %reshape.900), calls=%async_computation.3 | async-start | bytes 1048576 | tf_op jit(solution)/shard_map/all_to_all | solution.py:261
  353.4 11.6 %copy-start.7 = (bf16[32,2048]{1,0:T(8,128)(2,1)S(1)}, bf16[32,2048]{1,0:T(8,128)(2,1)}, u32[]{:S(2)}) copy-start(bf16[32,2048]{1,0:T(8,128)(2,1)} %reduce-scatter.3.cloned.1.call-done) | copy-start | bytes 393220
  (3 other events, 3.6 us)
Sparse Core Ops, SparseCore 0:
  36.0 28.4 all-gather.16
  74.5 28.0 all-gather.12
  144.2 60.3 reduce-scatter.2
  224.3 40.1 all-gather.14
  280.3 63.8 reduce-scatter.4
where the time goes:
time: 374 us; the launch traced here: 372 us
  waiting for transfers between devices  172 us (46%)
  between operations  55.8 us (15%)
  blocking collectives  51.8 us (14%)
  matrix products  30.8 us (8%)
  local copies, waits for them, and re-layouts  25.3 us (7%)
  other arithmetic  23.4 us (6%)
  starting transfers between devices  7.62 us (2%)
  loops' own time  5.4 us (1%)
    reduce_scatter x1, waiting for transfers between devices, on_device(): lax.psum_scatter(jnp.dot(hidden, down_proj[0], preferred_element_type=jnp...  63.2 us
    reduce_scatter x1, waiting for transfers between devices, on_device(): lax.psum_scatter(jnp.dot(head_rows, out_weight, preferred_element_type=jn...  59.9 us
    all_gather x1, waiting for transfers between devices, on_device(): piece = lax.all_gather(arrived, 'tp', axis=0, tiled=True)  40.1 us
    unnamed x2, blocking collectives  19.3 us
    all_gather x2, blocking collectives, carried_in(): pieces = jax.tree.map(lambda part: lax.all_gather(part, axis), running)  16.6 us
    all_to_all x1, blocking collectives, on_device(): lax.all_to_all(outgoing, SP, split_axis=0, concat_axis=0, tiled=True)  15.9 us
    dot_general x1, matrix products, on_device(): jnp.dot(hidden, down_proj[0], preferred_element_type=jnp.float32)  10.6 us
    unnamed x49, local copies, waits for them, and re-layouts  9.59 us
  transfers between devices with their start and end apart: 6, of which 4 were waited for; matrix products, arithmetic and copies ran while one was open for 7% of the time, Pallas kernels for 0%

commit v1 on v0

--- a/solution.py
+++ b/solution.py
@@ -247,7 +247,9 @@
     arrived = lax.all_to_all(outgoing, SP, split_axis=0, concat_axis=0, tiled=True).reshape(
         -1, model_width
     )
-    piece = lax.all_gather(arrived, "tp", axis=0, tiled=True)
+    piece = jnp.concatenate(
+        lax.all_to_all(jnp.stack([arrived] * lax.axis_size("tp")), "tp", 0, 0), axis=0
+    )
     gate_part = jnp.dot(piece, gate_proj[0], preferred_element_type=jnp.float32)
     up_part = jnp.dot(piece, up_proj[0], preferred_element_type=jnp.float32)
     hidden = (jax.nn.silu(gate_part) * up_part).astype(jnp.bfloat16)

time: 374 us -> 453 us (1.21)
  blocking collectives: 51.8 us -> 174 us
  waiting for transfers between devices: 172 us -> 129 us
    all_to_all x0 -> x1, blocking collectives: none -> 123 us  [on_device(): lax.all_to_all(jnp.stack([arrived] * lax.axis_size('tp')), 'tp', 0, 0)]
    all_gather x1 -> x0, waiting for transfers between devices: 40.1 us -> none  [on_device(): piece = lax.all_gather(arrived, 'tp', axis=0, tiled=True)]
    unnamed x49 -> x51, local copies, waits for them, and re-layouts: 9.59 us -> 11.5 us
  transfers between devices with their start and end apart: 6 -> 5, of which waited for: 4 -> 3; matrix products, arithmetic and copies ran while one was open for 7% -> 5% of each run, Pallas kernels for 0% -> 0%
where the time goes in v1:
time: 453 us; the launch traced here: 452 us
  blocking collectives  174 us (38%)
  waiting for transfers between devices  129 us (28%)
  between operations  56.9 us (13%)
  matrix products  28.3 us (6%)
  local copies, waits for them, and re-layouts  27.2 us (6%)
  other arithmetic  23.3 us (5%)
  starting transfers between devices  7.39 us (2%)
  loops' own time  5.15 us (1%)
    all_to_all x1, blocking collectives, on_device(): lax.all_to_all(jnp.stack([arrived] * lax.axis_size('tp')), 'tp', 0, 0)  123 us
    reduce_scatter x1, waiting for transfers between devices, on_device(): lax.psum_scatter(jnp.dot(hidden, down_proj[0], preferred_element_type=jnp...  60.4 us
    reduce_scatter x1, waiting for transfers between devices, on_device(): lax.psum_scatter(jnp.dot(head_rows, out_weight, preferred_element_type=jn...  59.8 us
    unnamed x2, blocking collectives  19.5 us
    all_gather x2, blocking collectives, carried_in(): pieces = jax.tree.map(lambda part: lax.all_gather(part, axis), running)  16.5 us
    all_to_all x1, blocking collectives, on_device(): lax.all_to_all(outgoing, SP, split_axis=0, concat_axis=0, tiled=True)  15.6 us
    unnamed x51, local copies, waits for them, and re-layouts  11.5 us
    dot_general x1, matrix products, on_device(): jnp.dot(hidden, down_proj[0], preferred_element_type=jnp.float32)  10.6 us
  transfers between devices with their start and end apart: 5, of which 3 were waited for; matrix products, arithmetic and copies ran while one was open for 5% of the time, Pallas kernels for 0%

profile of v1, /device:TPU:2, one launch (start us, length us, event | category | flops | bytes accessed | tf_op | source)
XLA Modules:
  0.0 451.5 jit_solution(17857413104721283777)
XLA Ops:
  6.5 1.4 fusion.182
  10.1 24.6 %while.23 = (s32[]{:T(128)}, f32[1,256,256]{2,1,0:T(8,128)S(1)}, f32[1,256]{1,0:T(1,128)S(1)}, f32[1]{0:T(128)}, s32[]{:T(128)}, /*index=5*/f32[2,1,256,256]{3,2...) while((s32[]{:T(128)}, f32[1,256,256]{2,1,0:T(8,128)S(1)}, ...), condition=%wide.region_6.7_spmd.clone, body=%wide.region_0.6_spmd.clone.sunk | while | flops 641046528 | bytes 6349332 | solution.py:106
  15.7 1.8 fusion.223
  28.0 1.8 fusion.223
  45.4 9.9 %all-reduce.8 = (f32[4]{0:T(128)S(1)}, f32[4]{0:T(128)S(1)}, f32[4]{0:T(128)S(1)}, f32[4]{0:T(128)S(1)}) all-reduce(f32[4]{0:T(128)S(1)} %dynamic-update-slice, f32[4]{0:T(128)S(1)} %fusion.156, f32[4]{0:T(128)S(1)} %dynamic-update-slice.3, f32[4]{0:T(128)S(1)} %dynamic-update-slice.6), channel_id=1, replica_groups=mesh['sp_0'=4,'sp_1'=4,'tp'=16] {'sp_1'}, use_global_device_ids=true, to_apply=%add | all-reduce | flops 16 | bytes 128
  56.0 2.5 fusion.152
  72.9 2.0 fusion.70
  75.6 1.9 fusion.188
  83.3 9.6 %all-reduce.9 = (f32[4]{0:T(128)S(1)}, f32[4]{0:T(128)S(1)}, f32[4]{0:T(128)S(1)}, f32[4]{0:T(128)S(1)}) all-reduce(f32[4]{0:T(128)S(1)} %dynamic-update-slice.1, f32[4]{0:T(128)S(1)} %dynamic-update-slice.4, f32[4]{0:T(128)S(1)} %dynamic-update-slice.5, f32[4]{0:T(128)S(1)} %dynamic-update-slice.7), channel_id=2, replica_groups=mesh['sp_0'=4,'sp_1'=4,'tp'=16] {'sp_0'}, use_global_device_ids=true, to_apply=%add.1 | all-reduce | flops 16 | bytes 128
  121.8 9.5 %all-gather.8 = f32[4,1,256]{2,1,0:T(1,128)S(1)} all-gather(f32[1,1,256]{2,1,0:T(1,128)S(1)} %bitcast.325), channel_id=9, replica_groups=mesh['sp_0'=4,'sp_1'=4,'tp'=16] {'sp_1'}, dimensions={0}, use_global_device_ids=true | all-gather | bytes 5120 | tf_op jit(solution)/shard_map/all_gather | solution.py:25
  131.4 7.0 %all_gather.81 = f32[4,1,256]{2,1,0:T(1,128)S(1)} all-gather(f32[1,1,256]{2,1,0:T(1,128)S(1)} %get-tuple-element.176), channel_id=1, replica_groups=mesh['sp_0'=4,'sp_1'=4,'tp'=16] {'sp_0'}, dimensions={0}, use_global_device_ids=true | all-gather | bytes 5120 | tf_op jit(solution)/shard_map/all_gather | solution.py:25
  139.8 2.6 multiply_reduce_fusion.1
  142.4 2.2 convolution_convert_fusion.1
  145.3 59.8 %reduce-scatter.3.cloned.1.call-done = bf16[32,2048]{1,0:T(8,128)(2,1)} async-done(((bf16[512,2048]{1,0:T(8,128)(2,1)}), bf16[32,2048]{1,0:T(8,128)(2,1)}) %reduce-scatter.3.cloned.1.call-update) | async-done | bytes 131088 | tf_op jit(solution)/shard_map/reduce_scatter | solution.py:220
  207.8 15.6 %all_to_all.15 = bf16[16,5,2048]{2,1,0:T(8,128)(2,1)S(1)} all-to-all(bf16[16,5,2048]{2,1,0:T(8,128)(2,1)S(1)} %reshape.900), channel_id=1, replica_groups=mesh['sp_0'=4,'sp_1'=4,'tp'=16] {'sp_0','sp_1'}, dimensions={0} | all-to-all | bytes 655360 | tf_op jit(solution)/shard_map/all_to_all | solution.py:247
  224.3 122.5 %all_to_all.16 = bf16[16,80,2048]{2,1,0:T(8,128)(2,1)S(1)} all-to-all(bf16[16,80,2048]{2,1,0:T(8,128)(2,1)S(1)} %stack.3), channel_id=1, replica_groups=mesh['sp_0'=4,'sp_1'=4,'tp'=16] {'tp'}, dimensions={0} | all-to-all | bytes 10485760 | tf_op jit(solution)/shard_map/all_to_all | solution.py:251
  346.8 2.3 copy-done.6
  349.2 2.6 fusion.56
  351.8 10.6 %convolution_convert_fusion = bf16[1280,2048]{1,0:T(8,128)(2,1)} fusion(bf16[1280,2048]{1,0:T(8,128)(2,1)} %bitcast.315, f32[1280,256]{1,0:T(8,128)} %fusion.56, bf16[1,256,2048]{2,1,0:T(8,128)(2,1)S(1)} %copy-done, bf16[1,2048,256]{2,1,0:T(8,128)(2,1)S(1)} %copy-done.16), kind=kOutput, calls=%fused_computation.75 | convolution fusion | flops 2688942080 | bytes 13893632 | tf_op jit(solution)/shard_map/dot_general | solution.py:257
  363.1 60.4 %reduce-scatter.5.cloned.1.call-done = bf16[80,2048]{1,0:T(8,128)(2,1)} async-done(((bf16[1280,2048]{1,0:T(8,128)(2,1)}), bf16[80,2048]{1,0:T(8,128)(2,1)}) %reduce-scatter.5.cloned.1.call-update) | async-done | bytes 327696 | tf_op jit(solution)/shard_map/reduce_scatter | solution.py:256
  423.5 1.9 reshape.902
  425.4 7.3 %all-to-all-start.2 = ((bf16[16,5,2048]{2,1,0:T(8,128)(2,1)}), bf16[16,5,2048]{2,1,0:T(8,128)(2,1)S(1)}, u32[]{:S(2)}, u32[]{:S(2)}) async-start(bf16[16,5,2048]{2,1,0:T(8,128)(2,1)} %reshape.902), calls=%async_computation.4 | async-start | bytes 1048576 | tf_op jit(solution)/shard_map/all_to_all | solution.py:263
  432.7 8.7 %all-to-all-done.2 = bf16[16,5,2048]{2,1,0:T(8,128)(2,1)S(1)} async-done(((bf16[16,5,2048]{2,1,0:T(8,128)(2,1)}), bf16[16,5,2048]{2,1,0:T(8,128)(2,1)S(1)}, u32[]{:S(2)}, u32[]{:S(2)}) %all-to-all-start.2) | async-done | bytes 327712 | tf_op jit(solution)/shard_map/all_to_all | solution.py:263
  442.5 1.8 multiply_reduce_fusion
  (170 shorter events, 43.6 us)
Async XLA Ops:
  6.5 345.3 %copy-start = (bf16[1,256,2048]{2,1,0:T(8,128)(2,1)S(1)}, bf16[1,256,2048]{2,1,0:T(8,128)(2,1)}, u32[]{:S(2)}) copy-start(bf16[1,256,2048]{2,1,0:T(8,128)(2,1)} %param.31) | copy-start | bytes 3145732
  6.5 66.4 %all-gather.14.cloned.1.call-start = ((), (), s32[]{:S(2)}) async-start(), calls=%async_computation.8 | async-start | bytes 1310720 | tf_op jit(solution)/shard_map/all_gather | solution.py:25
  10.1 31.5 %copy-start.18 = (u32[256]{0:T(256)S(1)}, u32[256]{0:T(256)}, u32[]{:S(2)}) copy-start(u32[256]{0:T(256)} %constant.127) | copy-start | bytes 3076
  10.1 64.9 %copy-start.17 = (u32[256]{0:T(256)S(1)}, u32[256]{0:T(256)}, u32[]{:S(2)}) copy-start(u32[256]{0:T(256)} %constant.132) | copy-start | bytes 3076
  10.1 10.6 %copy-start.4 = (bf16[2,1,256,256]{3,2,1,0:T(8,128)(2,1)S(1)}, bf16[2,1,256,256]{3,2,1,0:T(8,128)(2,1)}, u32[]{:S(2)}) copy-start(bf16[2,1,256,256]{3,2,1,0:T(8,128)(2,1)} %get-tuple-element.388) | copy-start | bytes 786436 | tf_op jit(solution)/shard_map/vmap()/while
  10.1 10.6 %copy-start.5 = (bf16[2,1,256,256]{3,2,1,0:T(8,128)(2,1)S(1)}, bf16[2,1,256,256]{3,2,1,0:T(8,128)(2,1)}, u32[]{:S(2)}) copy-start(bf16[2,1,256,256]{3,2,1,0:T(8,128)(2,1)} %get-tuple-element.387) | copy-start | bytes 786436 | tf_op jit(solution)/shard_map/vmap()/while
  10.1 11.1 %copy-start.2 = (bf16[2,1,256,256]{3,2,1,0:T(8,128)(2,1)S(1)}, bf16[2,1,256,256]{3,2,1,0:T(8,128)(2,1)}, u32[]{:S(2)}) copy-start(bf16[2,1,256,256]{3,2,1,0:T(8,128)(2,1)} %get-tuple-element.389) | copy-start | bytes 786436 | tf_op jit(solution)/shard_map/vmap()/while
  22.4 10.6 %copy-start.4 = (bf16[2,1,256,256]{3,2,1,0:T(8,128)(2,1)S(1)}, bf16[2,1,256,256]{3,2,1,0:T(8,128)(2,1)}, u32[]{:S(2)}) copy-start(bf16[2,1,256,256]{3,2,1,0:T(8,128)(2,1)} %get-tuple-element.388) | copy-start | bytes 786436 | tf_op jit(solution)/shard_map/vmap()/while
  22.4 10.6 %copy-start.5 = (bf16[2,1,256,256]{3,2,1,0:T(8,128)(2,1)S(1)}, bf16[2,1,256,256]{3,2,1,0:T(8,128)(2,1)}, u32[]{:S(2)}) copy-start(bf16[2,1,256,256]{3,2,1,0:T(8,128)(2,1)} %get-tuple-element.387) | copy-start | bytes 786436 | tf_op jit(solution)/shard_map/vmap()/while
  22.4 11.1 %copy-start.2 = (bf16[2,1,256,256]{3,2,1,0:T(8,128)(2,1)S(1)}, bf16[2,1,256,256]{3,2,1,0:T(8,128)(2,1)}, u32[]{:S(2)}) copy-start(bf16[2,1,256,256]{3,2,1,0:T(8,128)(2,1)} %get-tuple-element.389) | copy-start | bytes 786436 | tf_op jit(solution)/shard_map/vmap()/while
  34.7 103.6 %copy-start.10 = (s32[512]{0:T(512)S(1)}, s32[512]{0:T(512)}, u32[]{:S(2)}) copy-start(s32[512]{0:T(512)} %param.23) | copy-start | bytes 6148
  34.7 104.4 %copy-start.3 = (bf16[2,1,256,256]{3,2,1,0:T(8,128)(2,1)S(1)}, bf16[2,1,256,256]{3,2,1,0:T(8,128)(2,1)}, u32[]{:S(2)}) copy-start(bf16[2,1,256,256]{3,2,1,0:T(8,128)(2,1)} %get-tuple-element.403) | copy-start | bytes 786436
  35.5 104.3 %all-gather.12.cloned.1.call-start = ((), (), s32[]{:S(2)}) async-start(), calls=%async_computation.5 | async-start | bytes 1310720 | tf_op jit(solution)/shard_map/all_gather | solution.py:25
  75.0 130.1 %reduce-scatter.3.cloned.1.call-start = ((), (), s32[]{:S(2)}) async-start(), calls=%async_computation.6 | async-start | bytes 2228224 | tf_op jit(solution)/shard_map/reduce_scatter | solution.py:220
  139.8 2.6 copy-start.9
  139.8 2.6 copy-start.14
  142.4 62.7 %copy-start.7 = (bf16[32,2048]{1,0:T(8,128)(2,1)S(1)}, bf16[32,2048]{1,0:T(8,128)(2,1)}, u32[]{:S(2)}) copy-start(bf16[32,2048]{1,0:T(8,128)(2,1)} %param.17) | copy-start | bytes 393220
  144.6 61.6 %copy-start.12 = (f32[2048]{0:T(1024)S(1)}, f32[2048]{0:T(1024)}, u32[]{:S(2)}) copy-start(f32[2048]{0:T(1024)} %param.26) | copy-start | bytes 24580
  144.6 278.9 %reduce-scatter.5.cloned.1.call-start = ((), (), s32[]{:S(2)}) async-start(), calls=%async_computation.7 | async-start | bytes 5570560 | tf_op jit(solution)/shard_map/reduce_scatter | solution.py:256
  224.3 124.9 %copy-start.15 = (bf16[1,2048,256]{2,1,0:T(8,128)(2,1)S(1)}, bf16[1,2048,256]{2,1,0:T(8,128)(2,1)}, u32[]{:S(2)}) copy-start(bf16[1,2048,256]{2,1,0:T(8,128)(2,1)} %param.29) | copy-start | bytes 3145732
  346.8 2.3 copy-start.6
  349.2 2.6 copy-start.16
  425.4 16.0 %all-to-all-start.2 = ((bf16[16,5,2048]{2,1,0:T(8,128)(2,1)}), bf16[16,5,2048]{2,1,0:T(8,128)(2,1)S(1)}, u32[]{:S(2)}, u32[]{:S(2)}) async-start(bf16[16,5,2048]{2,1,0:T(8,128)(2,1)} %reshape.902), calls=%async_computation.4 | async-start | bytes 1048576 | tf_op jit(solution)/shard_map/all_to_all | solution.py:263
  432.7 11.6 %copy-start.8 = (bf16[32,2048]{1,0:T(8,128)(2,1)S(1)}, bf16[32,2048]{1,0:T(8,128)(2,1)}, u32[]{:S(2)}) copy-start(bf16[32,2048]{1,0:T(8,128)(2,1)} %reduce-scatter.3.cloned.1.call-done) | copy-start | bytes 393220
  (3 other events, 3.7 us)
Sparse Core Ops, SparseCore 0:
  35.6 28.4 all-gather.13
  75.1 28.0 all-gather.11
  144.8 60.2 reduce-scatter.2
  362.5 60.9 reduce-scatter.4
